TPU v7x, 128 devices: a whole 4x4x4 slice. The times are simulated.
128 devices in a mesh: fs: 16 (over z, y), tp: 8 (over x, core).
Axes of the slice: x: 4, y: 4, z: 4, core: 2. Of those that a mesh axis runs over, the one named last changes fastest.
Arguments:
- saved_input: bfloat16 [262144, 2048], P(('fs', 'tp')), may hold values from -500 to 500
- value_cotangent: bfloat16 [262144, 1024], P(('fs', 'tp')), may hold values from -500 to 500
- hidden_input: bfloat16 [262144, 1024], P(('fs', 'tp')), may hold values from -500 to 500
- out_cotangent: bfloat16 [262144, 2048], P(('fs', 'tp')), may hold values from -500 to 500
- value_factor: bfloat16 [2048, 256], P('fs'), may hold values from -2 to 2
- out_factor: bfloat16 [1024, 256], P('fs'), may hold values from -2 to 2
- value_weight: float32 [2048, 1024], P('fs', 'tp'), may hold values from -0.125 to 0.125
- out_weight: float32 [1024, 2048], P('fs', 'tp'), may hold values from -0.1875 to 0.1875
- value_first: float32 [256, 1024], P('fs', 'tp'), may hold values from -1.2 to 1.2
- value_second: float32 [256, 1024], P('fs', 'tp'), may hold values from 0.02 to 0.5
- out_first: float32 [256, 2048], P('fs', 'tp'), may hold values from -1.2 to 1.2
- out_second: float32 [256, 2048], P('fs', 'tp'), may hold values from 0.02 to 0.5
Outputs:
- value_update: float32 [2048, 1024], P('fs', 'tp')
- out_update: float32 [1024, 2048], P('fs', 'tp')
- new_value_weight: float32 [2048, 1024], P('fs', 'tp')
- new_out_weight: float32 [1024, 2048], P('fs', 'tp')
- value_copy: bfloat16 [2048, 1024], P(None, 'tp')
- out_copy: bfloat16 [1024, 2048], P(None, 'tp')
- new_value_first: float32 [256, 1024], P('fs', 'tp')
- new_value_second: float32 [256, 1024], P('fs', 'tp')
- new_out_first: float32 [256, 2048], P('fs', 'tp')
- new_out_second: float32 [256, 2048], P('fs', 'tp')
All inputs are finite; a program needn't handle non-finite values.
Results may differ from a plain program's by a relative error of at most 0.0065.
Values may be sent and summed in bfloat16 or wider, within the bound.
No kernel may reach another device: no remote copies, remote signals or barrier semaphores. Data moves between devices by JAX's collectives and lax.ppermute only.
A program may use at most 128 MiB of HBM per device.

v0:
```python
import jax
import jax.numpy as jnp
from jax import lax
from jax.sharding import Mesh
from jax.sharding import PartitionSpec as P

D = 2048
DM = 1024
R = 256
FS = ("fs_0", "fs_1")
TP = ("tp_0", "tp_1")
FS_TP = ("fs_0", "fs_1", "tp_0", "tp_1")
momentum_decay = 0.9
square_decay = 0.95
adam_epsilon = 1e-08
update_scale = 0.25
learning_rate = 0.01


def copy_for_each(shard, axis):
    copies = jnp.broadcast_to(shard, (lax.axis_size(axis), *shard.shape))
    return lax.all_to_all(copies, axis, split_axis=0, concat_axis=0, tiled=True)


def laid_out(tiles, dim):
    tiles = jnp.moveaxis(tiles, 0, dim)
    lengths = tiles.shape
    return tiles.reshape(*lengths[:dim], lengths[dim] * lengths[dim + 1], *lengths[dim + 2 :])


def collect(shard, axis, dim):
    tiles = copy_for_each(shard, axis)
    return laid_out(tiles, dim)


def split_up(shard, dim, length):
    before, after = (shard.shape[:dim], shard.shape[dim + 1 :])
    return jnp.moveaxis(shard.reshape(*before, length, -1, *after), dim, 0)


def sum_at_owner(shard, axis, dim):
    length = lax.axis_size(axis)
    tiles = lax.all_to_all(split_up(shard, dim, length), axis, 0, 0, tiled=True)
    return jnp.sum(tiles.astype(jnp.float32), axis=0)


def sum_at_owner_2(shard, axis, dim):
    tiles = split_up(shard, dim, lax.axis_size(axis))
    arrived = lax.all_to_all(tiles, axis, split_axis=0, concat_axis=0, tiled=True)
    return arrived.sum(axis=0)


def over_axes(shard, axes):
    for axis in axes:
        shard = lax.psum(shard, axis)
    return shard


def side_by_side(arrays, axis, dim, along):
    ends, at = ([], 0)
    for a in arrays[:-1]:
        at += a.shape[along]
        ends.append(at)
    both = jnp.concatenate(arrays, axis=along)
    return tuple(jnp.split(lax.all_gather(both, axis, axis=dim, tiled=True), ends, axis=along))


def gather_packed(arrays, axis, dims):
    flat = jnp.concatenate([a.reshape(-1) for a in arrays])
    lines, at, outs = (lax.all_gather(flat, axis), 0, [])
    for a, dim in zip(arrays, dims):
        tiles = lines[:, at : at + a.size].reshape(-1, *a.shape)
        outs.append(laid_out(tiles, dim))
        at += a.size
    return tuple(outs)


def moment_ratio(first, second, lowrank, clip_factor):
    scaled = clip_factor * lowrank
    new_first = momentum_decay * first + (1.0 - momentum_decay) * scaled
    new_second = square_decay * second + (1.0 - square_decay) * scaled * scaled
    ratio = new_first / (jnp.sqrt(new_second) + adam_epsilon)
    return (new_first, new_second, ratio)


def input_times_factor(inputs, factor):
    return jnp.dot(inputs, collect(factor, FS, 0), preferred_element_type=jnp.float32)


def split_product(basis, cotangents):
    basis_high = basis.astype(jnp.bfloat16)
    basis_rest = (basis - basis_high.astype(jnp.float32)).astype(jnp.bfloat16)
    high_part = jnp.einsum("tr,tc->rc", basis_high, cotangents, preferred_element_type=jnp.float32)
    rest_part = jnp.einsum("tr,tc->rc", basis_rest, cotangents, preferred_element_type=jnp.float32)
    return high_part + rest_part


def shards(
    saved_input,
    value_cotangent,
    hidden_input,
    out_cotangent,
    value_factor,
    out_factor,
    value_weight,
    out_weight,
    value_first,
    value_second,
    out_first,
    out_second,
):
    highest = lax.Precision.HIGHEST
    value_basis = input_times_factor(saved_input, value_factor)
    out_basis = input_times_factor(hidden_input, out_factor)
    left = value_basis
    right = out_basis
    first_part = split_product(left, value_cotangent)
    second_part = split_product(right, out_cotangent)
    lowrank = sum_at_owner(
        jnp.concatenate([first_part, second_part], axis=1).astype(jnp.bfloat16), FS, 0
    )
    low_value, low_out = (
        sum_at_owner_2(lowrank[:, :DM], TP, 1),
        sum_at_owner_2(lowrank[:, DM:], TP, 1),
    )
    squares = (
        over_axes(jnp.sum(low_value * low_value), FS_TP),
        over_axes(jnp.sum(low_out * low_out), FS_TP),
    )
    root_mean = jnp.sqrt((squares[0] + squares[1]) / (R * (D + DM)))
    clip_factor = 1.0 / jnp.maximum(root_mean, 1.0)
    new_value_first, new_value_second, value_ratio = moment_ratio(
        value_first, value_second, low_value, clip_factor
    )
    new_out_first, new_out_second, out_ratio = moment_ratio(
        out_first, out_second, low_out, clip_factor
    )
    pieces = side_by_side((value_ratio, out_ratio), FS, 0, 1)
    left = value_factor.astype(jnp.float32)
    right = out_factor.astype(jnp.float32)
    value_sum = jnp.dot(left, pieces[0], precision=highest)
    out_sum = jnp.dot(right, pieces[1], precision=highest)
    value_update = update_scale * value_sum
    out_update = update_scale * out_sum
    new_value_weight = value_weight - learning_rate * value_update
    new_out_weight = out_weight - learning_rate * out_update
    value_copy, out_copy = gather_packed(
        (new_value_weight.astype(jnp.bfloat16), new_out_weight.astype(jnp.bfloat16)), FS, (0, 0)
    )
    return (
        value_update,
        out_update,
        new_value_weight,
        new_out_weight,
        value_copy,
        out_copy,
        new_value_first,
        new_value_second,
        new_out_first,
        new_out_second,
    )


def solution(mesh):
    torus = Mesh(mesh.devices.reshape(4, 4, 4, 2), ("fs_0", "fs_1", "tp_0", "tp_1"))
    return jax.shard_map(
        shards,
        mesh=torus,
        in_specs=(
            P(FS_TP, None),
            P(FS_TP, None),
            P(FS_TP, None),
            P(FS_TP, None),
            P(FS, None),
            P(FS, None),
            P(FS, TP),
            P(FS, TP),
            P(FS, TP),
            P(FS, TP),
            P(FS, TP),
            P(FS, TP),
        ),
        out_specs=(
            P(FS, TP),
            P(FS, TP),
            P(FS, TP),
            P(FS, TP),
            P(None, TP),
            P(None, TP),
            P(FS, TP),
            P(FS, TP),
            P(FS, TP),
            P(FS, TP),
        ),
        check_vma=False,
    )
```

profile of v0, /device:TPU:0, one launch (start us, length us, event | category | flops | bytes accessed | tf_op | source)
XLA Modules:
  0.0 212.2 jit_solution(17302194149277601238)
XLA Ops:
  8.0 19.5 %all_to_all.25 = bf16[16,64,256]{2,1,0:T(8,128)(2,1)S(1)} all-to-all(bf16[16,64,256]{2,1,0:T(8,128)(2,1)S(1)} %broadcast_in_dim.7), channel_id=1, replica_groups=mesh['fs_0'=4,'fs_1'=4,'tp_0'=4,'tp_1'=2] {'fs_0','fs_1'}, dimensions={0} | all-to-all | bytes 1048576 | tf_op jit(solution)/shard_map/all_to_all | solution.py:22
  27.5 1.9 broadcast_in_dim.6
  29.4 3.7 %all-to-all-start = ((bf16[16,128,256]{2,1,0:T(8,128)(2,1)}), bf16[16,128,256]{2,1,0:T(8,128)(2,1)S(1)}, u32[]{:S(2)}, u32[]{:S(2)}) async-start(bf16[16,128,256]{2,1,0:T(8,128)(2,1)} %broadcast_in_dim.6), calls=%async_computation | async-start | bytes 2097152 | tf_op jit(solution)/shard_map/all_to_all | solution.py:22
  33.1 3.6 %fusion.19 = f32[2048,256]{1,0:T(8,128)S(1)} fusion(bf16[2048,1024]{1,0:T(8,128)(2,1)} %param.14, bf16[1024,256]{1,0:T(8,128)(2,1)S(1)} %bitcast.41), kind=kOutput, calls=%fused_computation.39 | convolution fusion | flops 1073741824 | bytes 6815744 | tf_op jit(solution)/shard_map/dot_general | solution.py:87
  36.7 5.9 %fusion.3 = f32[256,2048]{1,0:T(8,128)S(1)} fusion(bf16[2048,2048]{1,0:T(8,128)(2,1)} %param.15, f32[2048,256]{1,0:T(8,128)S(1)} %fusion.19), kind=kOutput, calls=%fused_computation.9 | convolution fusion | flops 2148007936 | bytes 12582912 | tf_op jit(solution)/shard_map/tr,tc->rc/dot_general | solution.py:93
  42.6 2.4 %fusion = bf16[256,2048]{1,0:T(8,128)(2,1)S(1)} fusion(f32[256,2048]{1,0:T(8,128)S(1)} %fusion.3, bf16[2048,2048]{1,0:T(8,128)(2,1)S(1)} %bitcast.38, f32[2048,256]{1,0:T(8,128)S(1)} %fusion.19), kind=kOutput, calls=%fused_computation.2 | convolution fusion | flops 2150629376 | bytes 13631488 | tf_op jit(solution)/shard_map/tr,tc->rc/dot_general | solution.py:94
  45.0 4.4 %all-to-all-done = bf16[16,128,256]{2,1,0:T(8,128)(2,1)S(1)} async-done(((bf16[16,128,256]{2,1,0:T(8,128)(2,1)}), bf16[16,128,256]{2,1,0:T(8,128)(2,1)S(1)}, u32[]{:S(2)}, u32[]{:S(2)}) %all-to-all-start) | async-done | bytes 1048608 | tf_op jit(solution)/shard_map/all_to_all | solution.py:22
  49.4 6.0 %fusion.18 = f32[2048,256]{1,0:T(8,128)S(1)} fusion(bf16[2048,2048]{1,0:T(8,128)(2,1)} %param.12, bf16[2048,256]{1,0:T(8,128)(2,1)S(1)} %bitcast.40), kind=kOutput, calls=%fused_computation.38 | convolution fusion | flops 2147483648 | bytes 11534336 | tf_op jit(solution)/shard_map/dot_general | solution.py:87
  55.4 1.3 fusion.6
  56.7 1.3 fusion.1
  58.1 25.1 %all_to_all.26 = bf16[16,16,3072]{2,1,0:T(8,128)(2,1)S(1)} all-to-all(bf16[16,16,3072]{2,1,0:T(8,128)(2,1)S(1)} %pad_maximum_fusion), channel_id=1, replica_groups=mesh['fs_0'=4,'fs_1'=4,'tp_0'=4,'tp_1'=2] {'fs_0','fs_1'}, dimensions={0} | all-to-all | bytes 3145728 | tf_op jit(solution)/shard_map/all_to_all | solution.py:43
  84.2 4.3 %all-to-all-start.3 = ((f32[8,16,128]{2,1,0:T(8,128)}), f32[8,16,128]{2,1,0:T(8,128)S(1)}, u32[]{:S(2)}, u32[]{:S(2)}) async-start(f32[8,16,128]{2,1,0:T(8,128)} %copy.33), calls=%async_computation.3 | async-start | bytes 131072 | tf_op jit(solution)/shard_map/all_to_all | solution.py:49
  89.2 4.9 %all-to-all-done.3 = f32[8,16,128]{2,1,0:T(8,128)S(1)} async-done(((f32[8,16,128]{2,1,0:T(8,128)}), f32[8,16,128]{2,1,0:T(8,128)S(1)}, u32[]{:S(2)}, u32[]{:S(2)}) %all-to-all-start.3) | async-done | bytes 65568 | tf_op jit(solution)/shard_map/all_to_all | solution.py:49
  94.1 3.4 %all-to-all-start.4 = ((f32[8,16,256]{2,1,0:T(8,128)}), f32[8,16,256]{2,1,0:T(8,128)S(1)}, u32[]{:S(2)}, u32[]{:S(2)}) async-start(f32[8,16,256]{2,1,0:T(8,128)} %copy.34), calls=%async_computation.4 | async-start | bytes 262144 | tf_op jit(solution)/shard_map/all_to_all | solution.py:49
  98.1 5.4 %all-to-all-done.4 = f32[8,16,256]{2,1,0:T(8,128)S(1)} async-done(((f32[8,16,256]{2,1,0:T(8,128)}), f32[8,16,256]{2,1,0:T(8,128)S(1)}, u32[]{:S(2)}, u32[]{:S(2)}) %all-to-all-start.4) | async-done | bytes 131104 | tf_op jit(solution)/shard_map/all_to_all | solution.py:49
  105.4 9.1 %psum.67 = f32[]{:T(128)} all-reduce(f32[]{:T(128)S(6)} %add.51), channel_id=1, replica_groups=mesh['fs_0'=4,'fs_1'=4,'tp_0'=4,'tp_1'=2] {'fs_0'}, use_global_device_ids=true, to_apply=%region_3.0 | all-reduce | flops 1 | bytes 8 | tf_op jit(solution)/shard_map/psum | solution.py:55
  114.5 9.2 %psum.66 = f32[]{:T(128)} all-reduce(f32[]{:T(128)} %psum.67), channel_id=1, replica_groups=mesh['fs_0'=4,'fs_1'=4,'tp_0'=4,'tp_1'=2] {'fs_1'}, use_global_device_ids=true, to_apply=%region_4.0 | all-reduce | flops 1 | bytes 8 | tf_op jit(solution)/shard_map/psum | solution.py:55
  123.7 9.5 %psum.65 = f32[]{:T(128)} all-reduce(f32[]{:T(128)} %psum.66), channel_id=1, replica_groups=mesh['fs_0'=4,'fs_1'=4,'tp_0'=4,'tp_1'=2] {'tp_0'}, use_global_device_ids=true, to_apply=%region_5.0 | all-reduce | flops 1 | bytes 8 | tf_op jit(solution)/shard_map/psum | solution.py:55
  133.3 3.1 %psum.64 = f32[]{:T(128)} all-reduce(f32[]{:T(128)} %psum.65), channel_id=1, replica_groups=mesh['fs_0'=4,'fs_1'=4,'tp_0'=4,'tp_1'=2] {'tp_1'}, use_global_device_ids=true, to_apply=%region_6.0 | all-reduce | flops 1 | bytes 8 | tf_op jit(solution)/shard_map/psum | solution.py:55
  138.4 22.0 %all_gather.9 = f32[256,384]{1,0:T(8,128)S(1)} all-gather(f32[16,384]{1,0:T(8,128)S(1)} %pad_maximum_fusion.2), channel_id=1, replica_groups=mesh['fs_0'=4,'fs_1'=4,'tp_0'=4,'tp_1'=2] {'fs_0','fs_1'}, dimensions={0}, use_global_device_ids=true | all-gather | bytes 417792 | tf_op jit(solution)/shard_map/all_gather | solution.py:65
  164.5 37.2 %all-gather.3.cloned.1.call-done = bf16[524288]{0:T(1024)(128)(2,1)} async-done(((bf16[32768]{0:T(1024)(128)(2,1)}), bf16[524288]{0:T(1024)(128)(2,1)}) %all-gather.3.cloned.1.call-update) | async-done | bytes 1048592 | tf_op jit(solution)/shard_map/all_gather | solution.py:70
  201.7 1.5 reshape.49
  203.3 1.0 reshape_reshape.6
  204.4 1.0 reshape_reshape.7
  (53 shorter events, 9.3 us)
Async XLA Ops:
  29.4 19.9 %all-to-all-start = ((bf16[16,128,256]{2,1,0:T(8,128)(2,1)}), bf16[16,128,256]{2,1,0:T(8,128)(2,1)S(1)}, u32[]{:S(2)}, u32[]{:S(2)}) async-start(bf16[16,128,256]{2,1,0:T(8,128)(2,1)} %broadcast_in_dim.6), calls=%async_computation | async-start | bytes 2097152 | tf_op jit(solution)/shard_map/all_to_all | solution.py:22
  33.1 9.5 %slice-start = ((s8[8388608]{0:T(1024)(128)(4,1)}), s8[4194304]{0:T(1024)(128)(4,1)S(1)}, s32[]{:S(2)}) async-start(s8[8388608]{0:T(1024)(128)(4,1)} %bitcast.37), calls=%async_computation.6 | async-start | bytes 8388608
  36.7 5.9 %slice-start.1 = ((s8[8388608]{0:T(1024)(128)(4,1)}), s8[4194304]{0:T(1024)(128)(4,1)S(1)}, s32[]{:S(2)}) async-start(s8[8388608]{0:T(1024)(128)(4,1)} %bitcast.37), calls=%async_computation.7 | async-start | bytes 8388608
  49.4 6.0 %copy-start.8 = (bf16[2048,1024]{1,0:T(8,128)(2,1)S(1)}, bf16[2048,1024]{1,0:T(8,128)(2,1)}, u32[]{:S(2)}) copy-start(bf16[2048,1024]{1,0:T(8,128)(2,1)} %param.13) | copy-start | bytes 12582916
  83.2 50.0 %copy-start.3 = (f32[128,128]{1,0:T(8,128)S(1)}, f32[128,128]{1,0:T(8,128)}, u32[]{:S(2)}) copy-start(f32[128,128]{1,0:T(8,128)} %param.18) | copy-start | bytes 196612
  83.2 53.9 %copy-start.4 = (f32[16,256]{1,0:T(8,128)S(1)}, f32[16,256]{1,0:T(8,128)}, u32[]{:S(2)}) copy-start(f32[16,256]{1,0:T(8,128)} %param.23) | copy-start | bytes 49156
  83.2 54.0 %copy-start.5 = (f32[16,256]{1,0:T(8,128)S(1)}, f32[16,256]{1,0:T(8,128)}, u32[]{:S(2)}) copy-start(f32[16,256]{1,0:T(8,128)} %param.22) | copy-start | bytes 49156
  83.2 54.6 %copy-start.6 = (f32[16,128]{1,0:T(8,128)S(1)}, f32[16,128]{1,0:T(8,128)}, u32[]{:S(2)}) copy-start(f32[16,128]{1,0:T(8,128)} %param.21) | copy-start | bytes 24580
  83.2 54.6 %copy-start.7 = (f32[16,128]{1,0:T(8,128)S(1)}, f32[16,128]{1,0:T(8,128)}, u32[]{:S(2)}) copy-start(f32[16,128]{1,0:T(8,128)} %param.20) | copy-start | bytes 24580
  83.2 77.1 %copy-start.1 = (bf16[64,256]{1,0:T(8,128)(2,1)S(1)}, bf16[64,256]{1,0:T(8,128)(2,1)}, u32[]{:S(2)}) copy-start(bf16[64,256]{1,0:T(8,128)(2,1)} %param.17) | copy-start | bytes 98308
  83.2 77.4 %copy-start = (bf16[128,256]{1,0:T(8,128)(2,1)S(1)}, bf16[128,256]{1,0:T(8,128)(2,1)}, u32[]{:S(2)}) copy-start(bf16[128,256]{1,0:T(8,128)(2,1)} %param.16) | copy-start | bytes 196612
  83.5 77.4 %copy-start.2 = (f32[64,256]{1,0:T(8,128)S(1)}, f32[64,256]{1,0:T(8,128)}, u32[]{:S(2)}) copy-start(f32[64,256]{1,0:T(8,128)} %param.19) | copy-start | bytes 196612
  84.2 9.9 %all-to-all-start.3 = ((f32[8,16,128]{2,1,0:T(8,128)}), f32[8,16,128]{2,1,0:T(8,128)S(1)}, u32[]{:S(2)}, u32[]{:S(2)}) async-start(f32[8,16,128]{2,1,0:T(8,128)} %copy.33), calls=%async_computation.3 | async-start | bytes 131072 | tf_op jit(solution)/shard_map/all_to_all | solution.py:49
  94.1 9.4 %all-to-all-start.4 = ((f32[8,16,256]{2,1,0:T(8,128)}), f32[8,16,256]{2,1,0:T(8,128)S(1)}, u32[]{:S(2)}, u32[]{:S(2)}) async-start(f32[8,16,256]{2,1,0:T(8,128)} %copy.34), calls=%async_computation.4 | async-start | bytes 262144 | tf_op jit(solution)/shard_map/all_to_all | solution.py:49
  97.5 104.3 %all-gather.3.cloned.1.call-start = ((), (), s32[]{:S(2)}) async-start(), calls=%async_computation.5 | async-start | bytes 1114112 | tf_op jit(solution)/shard_map/all_gather | solution.py:70
Sparse Core Ops, SparseCore 0:
  162.5 39.1 all-gather.2
where the time goes:
time: 213 us; the launch traced here: 212 us
  blocking collectives  97.5 us (46%)
  waiting for transfers between devices  51.9 us (24%)
  matrix products  20.9 us (10%)
  between operations  16.4 us (8%)
  starting transfers between devices  11.4 us (5%)
  local copies, waits for them, and re-layouts  9.54 us (4%)
  other arithmetic  4.73 us (2%)
    all_gather x1, waiting for transfers between devices, gather_packed(): lines, at, outs = (lax.all_gather(flat, axis), 0, [])  37.2 us
    psum x4, blocking collectives, over_axes(): shard = lax.psum(shard, axis)  30.9 us
    all_to_all x1, blocking collectives, sum_at_owner(): tiles = lax.all_to_all(split_up(shard, dim, length), axis, 0, 0, tiled=True)  25.1 us
    all_gather x1, blocking collectives, side_by_side(): lax.all_gather(both, axis, axis=dim, tiled=True)  22 us
    all_to_all x1, blocking collectives, copy_for_each(): return lax.all_to_all(copies, axis, split_axis=0, concat_axis=0, tiled=True)  19.5 us
    all_to_all x2, waiting for transfers between devices, sum_at_owner_2(): lax.all_to_all(tiles, axis, split_axis=0, concat_axis=0, tiled=True)  10.2 us
    dot_general x2, matrix products, input_times_factor(): jnp.dot(inputs, collect(factor, FS, 0), preferred_element_type=jnp.float32)  9.6 us
    all_to_all x2, starting transfers between devices, sum_at_owner_2(): lax.all_to_all(tiles, axis, split_axis=0, concat_axis=0, tiled=True)  7.67 us
  transfers between devices with their start and end apart: 4, of which 4 were waited for; matrix products, arithmetic and copies ran while one was open for 7% of the time, Pallas kernels for 0%

commit v1 on v0

--- a/solution.py
+++ b/solution.py
@@ -52,7 +52,8 @@
 
 def over_axes(shard, axes):
     for axis in axes:
-        shard = lax.psum(shard, axis)
+        parts = lax.all_gather(shard, axis)
+        shard = jnp.sum(parts, axis=0)
     return shard
 
 

time: 213 us -> 227 us (1.066)
  local copies, waits for them, and re-layouts: 9.54 us -> 23.1 us
  other arithmetic: 4.73 us -> 9.54 us
  blocking collectives: 97.5 us -> 95.2 us
    psum x4 -> x0, blocking collectives: 30.9 us -> none  [over_axes(): shard = lax.psum(shard, axis)]
    unnamed x0 -> x4, blocking collectives: none -> 28.6 us
    unnamed x29 -> x57, local copies, waits for them, and re-layouts: 1.7 us -> 15.3 us
    reduce_sum x0 -> x8, other arithmetic: none -> 4.81 us  [over_axes(): shard = jnp.sum(parts, axis=0)]
  transfers between devices with their start and end apart: 4 -> 4, of which waited for: 4 -> 4; matrix products, arithmetic and copies ran while one was open for 7% -> 8% of each run, Pallas kernels for 0% -> 0%
where the time goes in v1:
time: 227 us; the launch traced here: 226 us
  blocking collectives  95.2 us (42%)
  waiting for transfers between devices  49.9 us (22%)
  local copies, waits for them, and re-layouts  23.1 us (10%)
  matrix products  20.9 us (9%)
  between operations  15.8 us (7%)
  starting transfers between devices  11.4 us (5%)
  other arithmetic  9.54 us (4%)
    all_gather x1, waiting for transfers between devices, gather_packed(): lines, at, outs = (lax.all_gather(flat, axis), 0, [])  37.2 us
    unnamed x4, blocking collectives  28.6 us
    all_to_all x1, blocking collectives, sum_at_owner(): tiles = lax.all_to_all(split_up(shard, dim, length), axis, 0, 0, tiled=True)  25.2 us
    all_gather x1, blocking collectives, side_by_side(): lax.all_gather(both, axis, axis=dim, tiled=True)  22 us
    all_to_all x1, blocking collectives, copy_for_each(): return lax.all_to_all(copies, axis, split_axis=0, concat_axis=0, tiled=True)  19.5 us
    unnamed x57, local copies, waits for them, and re-layouts  15.3 us
    dot_general x2, matrix products, input_times_factor(): jnp.dot(inputs, collect(factor, FS, 0), preferred_element_type=jnp.float32)  9.59 us
    all_to_all x2, waiting for transfers between devices, sum_at_owner_2(): lax.all_to_all(tiles, axis, split_axis=0, concat_axis=0, tiled=True)  8.22 us
  transfers between devices with their start and end apart: 4, of which 4 were waited for; matrix products, arithmetic and copies ran while one was open for 8% of the time, Pallas kernels for 0%

profile of v1, /device:TPU:0, one launch (start us, length us, event | category | flops | bytes accessed | tf_op | source)
XLA Modules:
  0.0 225.8 jit_solution(3328762545576842187)
XLA Ops:
  8.0 19.5 %all_to_all.25 = bf16[16,64,256]{2,1,0:T(8,128)(2,1)S(1)} all-to-all(bf16[16,64,256]{2,1,0:T(8,128)(2,1)S(1)} %broadcast_in_dim.7), channel_id=1, replica_groups=mesh['fs_0'=4,'fs_1'=4,'tp_0'=4,'tp_1'=2] {'fs_0','fs_1'}, dimensions={0} | all-to-all | bytes 1048576 | tf_op jit(solution)/shard_map/all_to_all | solution.py:22
  27.5 1.9 broadcast_in_dim.6
  29.4 3.7 %all-to-all-start = ((bf16[16,128,256]{2,1,0:T(8,128)(2,1)}), bf16[16,128,256]{2,1,0:T(8,128)(2,1)S(1)}, u32[]{:S(2)}, u32[]{:S(2)}) async-start(bf16[16,128,256]{2,1,0:T(8,128)(2,1)} %broadcast_in_dim.6), calls=%async_computation | async-start | bytes 2097152 | tf_op jit(solution)/shard_map/all_to_all | solution.py:22
  33.1 3.6 %fusion.19 = f32[2048,256]{1,0:T(8,128)S(1)} fusion(bf16[2048,1024]{1,0:T(8,128)(2,1)} %param.14, bf16[1024,256]{1,0:T(8,128)(2,1)S(1)} %bitcast.53), kind=kOutput, calls=%fused_computation.39 | convolution fusion | flops 1073741824 | bytes 6815744 | tf_op jit(solution)/shard_map/dot_general | solution.py:88
  36.7 5.9 %fusion.3 = f32[256,2048]{1,0:T(8,128)S(1)} fusion(bf16[2048,2048]{1,0:T(8,128)(2,1)} %param.15, f32[2048,256]{1,0:T(8,128)S(1)} %fusion.19), kind=kOutput, calls=%fused_computation.9 | convolution fusion | flops 2148007936 | bytes 12582912 | tf_op jit(solution)/shard_map/tr,tc->rc/dot_general | solution.py:94
  42.6 2.4 %fusion = bf16[256,2048]{1,0:T(8,128)(2,1)S(1)} fusion(f32[256,2048]{1,0:T(8,128)S(1)} %fusion.3, bf16[2048,2048]{1,0:T(8,128)(2,1)S(1)} %bitcast.50, f32[2048,256]{1,0:T(8,128)S(1)} %fusion.19), kind=kOutput, calls=%fused_computation.2 | convolution fusion | flops 2150629376 | bytes 13631488 | tf_op jit(solution)/shard_map/tr,tc->rc/dot_general | solution.py:95
  45.0 4.4 %all-to-all-done = bf16[16,128,256]{2,1,0:T(8,128)(2,1)S(1)} async-done(((bf16[16,128,256]{2,1,0:T(8,128)(2,1)}), bf16[16,128,256]{2,1,0:T(8,128)(2,1)S(1)}, u32[]{:S(2)}, u32[]{:S(2)}) %all-to-all-start) | async-done | bytes 1048608 | tf_op jit(solution)/shard_map/all_to_all | solution.py:22
  49.4 6.0 %fusion.18 = f32[2048,256]{1,0:T(8,128)S(1)} fusion(bf16[2048,2048]{1,0:T(8,128)(2,1)} %param.12, bf16[2048,256]{1,0:T(8,128)(2,1)S(1)} %bitcast.52), kind=kOutput, calls=%fused_computation.38 | convolution fusion | flops 2147483648 | bytes 11534336 | tf_op jit(solution)/shard_map/dot_general | solution.py:88
  58.1 25.2 %all_to_all.26 = bf16[16,16,3072]{2,1,0:T(8,128)(2,1)S(1)} all-to-all(bf16[16,16,3072]{2,1,0:T(8,128)(2,1)S(1)} %pad_maximum_fusion), channel_id=1, replica_groups=mesh['fs_0'=4,'fs_1'=4,'tp_0'=4,'tp_1'=2] {'fs_0','fs_1'}, dimensions={0} | all-to-all | bytes 3145728 | tf_op jit(solution)/shard_map/all_to_all | solution.py:43
  84.2 4.3 %all-to-all-start.3 = ((f32[8,16,128]{2,1,0:T(8,128)}), f32[8,16,128]{2,1,0:T(8,128)S(1)}, u32[]{:S(2)}, u32[]{:S(2)}) async-start(f32[8,16,128]{2,1,0:T(8,128)} %copy.33), calls=%async_computation.3 | async-start | bytes 131072 | tf_op jit(solution)/shard_map/all_to_all | solution.py:49
  89.3 4.9 %all-to-all-done.3 = f32[8,16,128]{2,1,0:T(8,128)S(1)} async-done(((f32[8,16,128]{2,1,0:T(8,128)}), f32[8,16,128]{2,1,0:T(8,128)S(1)}, u32[]{:S(2)}, u32[]{:S(2)}) %all-to-all-start.3) | async-done | bytes 65568 | tf_op jit(solution)/shard_map/all_to_all | solution.py:49
  94.1 3.4 %all-to-all-start.4 = ((f32[8,16,256]{2,1,0:T(8,128)}), f32[8,16,256]{2,1,0:T(8,128)S(1)}, u32[]{:S(2)}, u32[]{:S(2)}) async-start(f32[8,16,256]{2,1,0:T(8,128)} %copy.34), calls=%async_computation.4 | async-start | bytes 262144 | tf_op jit(solution)/shard_map/all_to_all | solution.py:49
  100.2 3.4 %all-to-all-done.4 = f32[8,16,256]{2,1,0:T(8,128)S(1)} async-done(((f32[8,16,256]{2,1,0:T(8,128)}), f32[8,16,256]{2,1,0:T(8,128)S(1)}, u32[]{:S(2)}, u32[]{:S(2)}) %all-to-all-start.4) | async-done | bytes 131104 | tf_op jit(solution)/shard_map/all_to_all | solution.py:49
  106.1 8.6 %all-reduce.10 = (f32[4]{0:T(128)S(1)}, f32[4]{0:T(128)S(1)}) all-reduce(f32[4]{0:T(128)S(1)} %dynamic-update-slice, f32[4]{0:T(128)S(1)} %dynamic-update-slice.4), channel_id=1, replica_groups=mesh['fs_0'=4,'fs_1'=4,'tp_0'=4,'tp_1'=2] {'fs_0'}, use_global_device_ids=true, to_apply=%add | all-reduce | flops 8 | bytes 64
  115.9 1.4 dynamic-update-slice.1
  117.3 1.4 dynamic-update-slice.5
  119.3 8.8 %all-reduce.9 = (f32[4]{0:T(128)S(1)}, f32[4]{0:T(128)S(1)}) all-reduce(f32[4]{0:T(128)S(1)} %dynamic-update-slice.1, f32[4]{0:T(128)S(1)} %dynamic-update-slice.5), channel_id=1, replica_groups=mesh['fs_0'=4,'fs_1'=4,'tp_0'=4,'tp_1'=2] {'fs_1'}, use_global_device_ids=true, to_apply=%add.1 | all-reduce | flops 8 | bytes 64
  130.7 1.4 dynamic-update-slice.6
  132.7 8.9 %all-reduce.8 = (f32[4]{0:T(128)S(1)}, f32[4]{0:T(128)S(1)}) all-reduce(f32[4]{0:T(128)S(1)} %dynamic-update-slice.2, f32[4]{0:T(128)S(1)} %dynamic-update-slice.6), channel_id=1, replica_groups=mesh['fs_0'=4,'fs_1'=4,'tp_0'=4,'tp_1'=2] {'tp_0'}, use_global_device_ids=true, to_apply=%add.2 | all-reduce | flops 8 | bytes 64
  144.1 1.4 dynamic-update-slice.7
  145.6 2.5 %all-reduce.11 = (f32[2]{0:T(128)S(1)}, f32[2]{0:T(128)S(1)}) all-reduce(f32[2]{0:T(128)S(1)} %dynamic-update-slice.3, f32[2]{0:T(128)S(1)} %dynamic-update-slice.7), channel_id=1, replica_groups=mesh['fs_0'=4,'fs_1'=4,'tp_0'=4,'tp_1'=2] {'tp_1'}, use_global_device_ids=true, to_apply=%add.3 | all-reduce | flops 4 | bytes 32
  151.9 22.0 %all_gather.73 = f32[256,384]{1,0:T(8,128)S(1)} all-gather(f32[16,384]{1,0:T(8,128)S(1)} %pad_maximum_fusion.2), channel_id=1, replica_groups=mesh['fs_0'=4,'fs_1'=4,'tp_0'=4,'tp_1'=2] {'fs_0','fs_1'}, dimensions={0}, use_global_device_ids=true | all-gather | bytes 417792 | tf_op jit(solution)/shard_map/all_gather | solution.py:66
  178.0 37.2 %all-gather.3.cloned.1.call-done = bf16[524288]{0:T(1024)(128)(2,1)} async-done(((bf16[32768]{0:T(1024)(128)(2,1)}), bf16[524288]{0:T(1024)(128)(2,1)}) %all-gather.3.cloned.1.call-update) | async-done | bytes 1048592 | tf_op jit(solution)/shard_map/all_gather | solution.py:71
  215.3 1.5 reshape.49
  (89 shorter events, 26.7 us)
Async XLA Ops:
  29.4 19.9 %all-to-all-start = ((bf16[16,128,256]{2,1,0:T(8,128)(2,1)}), bf16[16,128,256]{2,1,0:T(8,128)(2,1)S(1)}, u32[]{:S(2)}, u32[]{:S(2)}) async-start(bf16[16,128,256]{2,1,0:T(8,128)(2,1)} %broadcast_in_dim.6), calls=%async_computation | async-start | bytes 2097152 | tf_op jit(solution)/shard_map/all_to_all | solution.py:22
  33.1 9.5 %slice-start = ((s8[8388608]{0:T(1024)(128)(4,1)}), s8[4194304]{0:T(1024)(128)(4,1)S(1)}, s32[]{:S(2)}) async-start(s8[8388608]{0:T(1024)(128)(4,1)} %bitcast.49), calls=%async_computation.6 | async-start | bytes 8388608
  36.7 5.9 %slice-start.1 = ((s8[8388608]{0:T(1024)(128)(4,1)}), s8[4194304]{0:T(1024)(128)(4,1)S(1)}, s32[]{:S(2)}) async-start(s8[8388608]{0:T(1024)(128)(4,1)} %bitcast.49), calls=%async_computation.7 | async-start | bytes 8388608
  49.4 6.0 %copy-start.8 = (bf16[2048,1024]{1,0:T(8,128)(2,1)S(1)}, bf16[2048,1024]{1,0:T(8,128)(2,1)}, u32[]{:S(2)}) copy-start(bf16[2048,1024]{1,0:T(8,128)(2,1)} %param.13) | copy-start | bytes 12582916
  83.2 14.4 %copy-start.12 = (u32[128]{0:T(128)S(1)}, u32[128]{0:T(128)}, u32[]{:S(2)}) copy-start(u32[128]{0:T(128)} %constant.8) | copy-start | bytes 1540
  83.2 22.3 %copy-start.11 = (u32[128]{0:T(128)S(1)}, u32[128]{0:T(128)}, u32[]{:S(2)}) copy-start(u32[128]{0:T(128)} %constant.37) | copy-start | bytes 1540
  83.2 35.5 %copy-start.10 = (u32[128]{0:T(128)S(1)}, u32[128]{0:T(128)}, u32[]{:S(2)}) copy-start(u32[128]{0:T(128)} %constant.42) | copy-start | bytes 1540
  83.2 48.9 %copy-start.9 = (u32[128]{0:T(128)S(1)}, u32[128]{0:T(128)}, u32[]{:S(2)}) copy-start(u32[128]{0:T(128)} %constant.47) | copy-start | bytes 1540
  83.2 62.3 %copy-start.3 = (f32[128,128]{1,0:T(8,128)S(1)}, f32[128,128]{1,0:T(8,128)}, u32[]{:S(2)}) copy-start(f32[128,128]{1,0:T(8,128)} %param.18) | copy-start | bytes 196612
  83.2 67.4 %copy-start.4 = (f32[16,256]{1,0:T(8,128)S(1)}, f32[16,256]{1,0:T(8,128)}, u32[]{:S(2)}) copy-start(f32[16,256]{1,0:T(8,128)} %param.23) | copy-start | bytes 49156
  83.2 67.4 %copy-start.5 = (f32[16,256]{1,0:T(8,128)S(1)}, f32[16,256]{1,0:T(8,128)}, u32[]{:S(2)}) copy-start(f32[16,256]{1,0:T(8,128)} %param.22) | copy-start | bytes 49156
  83.3 68.1 %copy-start.6 = (f32[16,128]{1,0:T(8,128)S(1)}, f32[16,128]{1,0:T(8,128)}, u32[]{:S(2)}) copy-start(f32[16,128]{1,0:T(8,128)} %param.21) | copy-start | bytes 24580
  83.3 68.1 %copy-start.7 = (f32[16,128]{1,0:T(8,128)S(1)}, f32[16,128]{1,0:T(8,128)}, u32[]{:S(2)}) copy-start(f32[16,128]{1,0:T(8,128)} %param.20) | copy-start | bytes 24580
  83.3 90.6 %copy-start.1 = (bf16[64,256]{1,0:T(8,128)(2,1)S(1)}, bf16[64,256]{1,0:T(8,128)(2,1)}, u32[]{:S(2)}) copy-start(bf16[64,256]{1,0:T(8,128)(2,1)} %param.17) | copy-start | bytes 98308
  83.3 90.8 %copy-start = (bf16[128,256]{1,0:T(8,128)(2,1)S(1)}, bf16[128,256]{1,0:T(8,128)(2,1)}, u32[]{:S(2)}) copy-start(bf16[128,256]{1,0:T(8,128)(2,1)} %param.16) | copy-start | bytes 196612
  83.5 90.9 %copy-start.2 = (f32[64,256]{1,0:T(8,128)S(1)}, f32[64,256]{1,0:T(8,128)}, u32[]{:S(2)}) copy-start(f32[64,256]{1,0:T(8,128)} %param.19) | copy-start | bytes 196612
  84.2 9.9 %all-to-all-start.3 = ((f32[8,16,128]{2,1,0:T(8,128)}), f32[8,16,128]{2,1,0:T(8,128)S(1)}, u32[]{:S(2)}, u32[]{:S(2)}) async-start(f32[8,16,128]{2,1,0:T(8,128)} %copy.33), calls=%async_computation.3 | async-start | bytes 131072 | tf_op jit(solution)/shard_map/all_to_all | solution.py:49
  94.1 9.4 %all-to-all-start.4 = ((f32[8,16,256]{2,1,0:T(8,128)}), f32[8,16,256]{2,1,0:T(8,128)S(1)}, u32[]{:S(2)}, u32[]{:S(2)}) async-start(f32[8,16,256]{2,1,0:T(8,128)} %copy.34), calls=%async_computation.4 | async-start | bytes 262144 | tf_op jit(solution)/shard_map/all_to_all | solution.py:49
  97.5 117.8 %all-gather.3.cloned.1.call-start = ((), (), s32[]{:S(2)}) async-start(), calls=%async_computation.5 | async-start | bytes 1114112 | tf_op jit(solution)/shard_map/all_gather | solution.py:71
Sparse Core Ops, SparseCore 0:
  176.0 39.1 all-gather.2
